TPU v7x, 32 devices: a whole 2x2x4 slice. The times are simulated.
32 devices in a mesh: sp: 4 (over z), dp: 8 (over y, x, core).
Axes of the slice: x: 2, y: 2, z: 4, core: 2. Of those that a mesh axis runs over, the one named last changes fastest.
Arguments:
- queries: bfloat16 [8, 512, 1024], P('dp', 'sp'), may hold values from -6 to 6
- key_rows: bfloat16 [8, 512, 1024], P('dp', 'sp'), may hold values from -6 to 6
- values: bfloat16 [8, 512, 2048], P('dp', 'sp'), may hold values from -6 to 6
- out_gate: bfloat16 [8, 512, 2048], P('dp', 'sp'), may hold values from -6 to 6
- input_gate: bfloat16 [8, 4, 512], P('dp', None, 'sp'), may hold values from -6 to 205
- forget_gate: bfloat16 [8, 4, 512], P('dp', None, 'sp'), may hold values from 0.5 to 13
- out_weight: bfloat16 [2048, 2048], P(None, 'dp'), may hold values from -0.125 to 0.125
Outputs:
- layer_out: bfloat16 [8, 512, 2048], P('dp', 'sp')
All inputs are finite; a program needn't handle non-finite values.
Results may differ from a plain program's by a relative error of at most 0.0057.
Values may be sent and summed in bfloat16 or wider, within the bound.
A program may use at most 64 MiB of HBM per device.

v0:
```python
import jax
import jax.numpy as jnp
from jax import lax
from jax.sharding import PartitionSpec as P

BLOCK = 128


def memory_cell(query_rows, key_in, value_rows, input_log, forget_log):
    block_count = query_rows.shape[0] // BLOCK
    key_width = query_rows.shape[1]
    value_width = value_rows.shape[1]
    key_scale = key_width ** (-0.5)
    causal = lax.broadcasted_iota(jnp.int32, (BLOCK, BLOCK), 0) >= lax.broadcasted_iota(
        jnp.int32, (BLOCK, BLOCK), 1
    )
    highest = lax.Precision.HIGHEST

    def block_step(state_in, inputs):
        memory, normer, stabil = state_in
        query_part, key_part, value_part, gain_part, decay_part = inputs
        query_part = query_part.astype(jnp.float32)
        key_part = key_part.astype(jnp.float32) * key_scale
        value_part = value_part.astype(jnp.float32)
        running = jnp.cumsum(decay_part)
        log_weight = running[:, None] - running[None, :] + gain_part[None, :]
        log_weight = jnp.where(causal, log_weight, -jnp.inf)
        carried_log = running + stabil
        row_top = jnp.maximum(carried_log, jnp.max(log_weight, axis=1))
        scores = jnp.dot(query_part, key_part.T, precision=highest) * jnp.exp(
            log_weight - row_top[:, None]
        )
        carried = jnp.exp(carried_log - row_top)
        numerator = jnp.dot(scores, value_part, precision=highest) + carried[:, None] * jnp.dot(
            query_part, memory, precision=highest
        )
        denominator = jnp.sum(scores, axis=1) + carried * jnp.dot(
            query_part, normer, precision=highest
        )
        output = numerator / jnp.maximum(jnp.abs(denominator), 1.0)[:, None]
        block_end = running[-1]
        weight_log = block_end - running + gain_part
        new_top = jnp.maximum(block_end + stabil, jnp.max(weight_log))
        weights = jnp.exp(weight_log - new_top)
        retain = jnp.exp(block_end + stabil - new_top)
        memory = retain * memory + jnp.dot(
            (key_part * weights[:, None]).T, value_part, precision=highest
        )
        normer = retain * normer + jnp.dot(weights, key_part, precision=highest)
        return ((memory, normer, new_top), output)

    start_state = (
        jnp.zeros((key_width, value_width), jnp.float32),
        jnp.zeros((key_width,), jnp.float32),
        jnp.zeros((), jnp.float32),
    )
    blocks = tuple(
        (
            source.reshape((block_count, BLOCK) + source.shape[1:])
            for source in (query_rows, key_in, value_rows, input_log, forget_log)
        )
    )
    _, outputs = lax.scan(block_step, start_state, blocks)
    return outputs.reshape(block_count * BLOCK, value_width)


def body(queries, key_rows, values, out_gate, input_gate, forget_gate, out_weight):
    group_count = lax.axis_size("sp")
    token_count = queries.shape[1]
    head_count = input_gate.shape[1]
    copies = group_count // head_count
    head_key = queries.shape[2] // head_count
    slice_width = values.shape[2] // group_count

    def spread(source):
        widened = jnp.broadcast_to(
            source[0].reshape(token_count, head_count, 1, head_key),
            (token_count, head_count, copies, head_key),
        )
        return widened.reshape(token_count, group_count, head_key)

    def spread_gate(source):
        return jnp.repeat(source[0].T, copies, axis=1)

    query_all, key_all = (
        lax.all_to_all(spread(queries), "sp", split_axis=1, concat_axis=0, tiled=True),
        lax.all_to_all(spread(key_rows), "sp", split_axis=1, concat_axis=0, tiled=True),
    )
    value_all, input_all, forget_all = (
        lax.all_to_all(
            values[0].reshape(token_count, group_count, slice_width),
            "sp",
            split_axis=1,
            concat_axis=0,
            tiled=True,
        ),
        lax.all_to_all(spread_gate(input_gate), "sp", split_axis=1, concat_axis=0, tiled=True),
        lax.all_to_all(spread_gate(forget_gate), "sp", split_axis=1, concat_axis=0, tiled=True),
    )
    output = memory_cell(
        query_all[:, 0],
        key_all[:, 0],
        value_all[:, 0],
        input_all[:, 0].astype(jnp.float32),
        jax.nn.log_sigmoid(forget_all[:, 0].astype(jnp.float32)),
    )
    hidden = output.astype(jnp.bfloat16)
    token_rows = lax.all_to_all(hidden, "sp", split_axis=0, concat_axis=1, tiled=True)
    gated_rows = (
        token_rows.astype(jnp.float32) * jax.nn.sigmoid(out_gate[0].astype(jnp.float32))
    ).astype(jnp.bfloat16)
    projected = jnp.dot(
        gated_rows,
        lax.all_gather(out_weight, "dp", axis=1, tiled=True),
        preferred_element_type=jnp.float32,
    )
    return projected.astype(jnp.bfloat16)[None]


def solution(mesh):
    return jax.shard_map(
        body,
        mesh=mesh,
        in_specs=(
            P("dp", "sp", None),
            P("dp", "sp", None),
            P("dp", "sp", None),
            P("dp", "sp", None),
            P("dp", None, "sp"),
            P("dp", None, "sp"),
            P(None, "dp"),
        ),
        out_specs=P("dp", "sp", None),
        check_vma=False,
    )
```

profile of v0, /device:TPU:0, one launch (start us, length us, event | category | flops | bytes accessed | tf_op | source)
XLA Modules:
  0.0 121.6 jit_solution(9997319030571958665)
XLA Ops:
  6.5 0.7 all-gather.2.cloned.1.call-update
  7.3 1.3 %copy.28 = bf16[128,4,1]{0,2,1:T(2,128)(2,1)} copy(bf16[128,4,1]{0,1,2:T(4,128)(2,1)} %bitcast.152) | data formatting | bytes 2048 | tf_op jit(solution)/shard_map/all_to_all | solution.py:98
  8.5 6.3 %all-to-all-start = ((bf16[128,4,1]{0,2,1:T(2,128)(2,1)}), bf16[128,4,1]{0,2,1:T(2,128)(2,1)S(1)}, u32[]{:S(2)}, u32[]{:S(2)}) async-start(bf16[128,4,1]{0,2,1:T(2,128)(2,1)} %copy.28), calls=%async_computation | async-start | bytes 4096 | tf_op jit(solution)/shard_map/all_to_all | solution.py:98
  14.9 1.3 %copy.29 = bf16[128,4,1]{0,2,1:T(2,128)(2,1)} copy(bf16[128,4,1]{0,1,2:T(4,128)(2,1)} %bitcast.153) | data formatting | bytes 2048 | tf_op jit(solution)/shard_map/all_to_all | solution.py:97
  16.1 4.2 %all-to-all-done = bf16[128,4,1]{0,2,1:T(2,128)(2,1)S(1)} async-done(((bf16[128,4,1]{0,2,1:T(2,128)(2,1)}), bf16[128,4,1]{0,2,1:T(2,128)(2,1)S(1)}, u32[]{:S(2)}, u32[]{:S(2)}) %all-to-all-start) | async-done | bytes 1056 | tf_op jit(solution)/shard_map/all_to_all | solution.py:98
  20.4 3.2 %all-to-all-start.1 = ((bf16[128,4,1]{0,2,1:T(2,128)(2,1)}), bf16[128,4,1]{0,2,1:T(2,128)(2,1)S(1)}, u32[]{:S(2)}, u32[]{:S(2)}) async-start(bf16[128,4,1]{0,2,1:T(2,128)(2,1)} %copy.29), calls=%async_computation.1 | async-start | bytes 4096 | tf_op jit(solution)/shard_map/all_to_all | solution.py:97
  23.6 1.8 %copy.30 = bf16[1,128,1024]{1,2,0:T(8,128)(2,1)} copy(bf16[1,128,1024]{2,1,0:T(8,128)(2,1)} %param.10) | data formatting | bytes 524288 | tf_op args[1]
  25.4 3.6 %all-to-all-done.1 = bf16[128,4,1]{0,2,1:T(2,128)(2,1)S(1)} async-done(((bf16[128,4,1]{0,2,1:T(2,128)(2,1)}), bf16[128,4,1]{0,2,1:T(2,128)(2,1)S(1)}, u32[]{:S(2)}, u32[]{:S(2)}) %all-to-all-start.1) | async-done | bytes 1056 | tf_op jit(solution)/shard_map/all_to_all | solution.py:97
  29.0 3.4 %all-to-all-start.2 = ((bf16[128,4,256]{0,2,1:T(8,128)(2,1)}), bf16[128,4,256]{0,2,1:T(8,128)(2,1)S(1)}, u32[]{:S(2)}, u32[]{:S(2)}) async-start(bf16[128,4,256]{0,2,1:T(8,128)(2,1)} %bitcast.11), calls=%async_computation.2 | async-start | bytes 524288 | tf_op jit(solution)/shard_map/all_to_all | solution.py:87
  32.4 1.8 %copy.32 = bf16[1,128,1024]{1,2,0:T(8,128)(2,1)} copy(bf16[1,128,1024]{2,1,0:T(8,128)(2,1)} %param.9) | data formatting | bytes 524288 | tf_op args[0]
  34.2 4.9 %all-to-all-done.2 = bf16[128,4,256]{0,2,1:T(8,128)(2,1)S(1)} async-done(((bf16[128,4,256]{0,2,1:T(8,128)(2,1)}), bf16[128,4,256]{0,2,1:T(8,128)(2,1)S(1)}, u32[]{:S(2)}, u32[]{:S(2)}) %all-to-all-start.2) | async-done | bytes 262176 | tf_op jit(solution)/shard_map/all_to_all | solution.py:87
  39.1 3.4 %all-to-all-start.4 = ((bf16[128,4,256]{0,2,1:T(8,128)(2,1)}), bf16[128,4,256]{0,2,1:T(8,128)(2,1)S(1)}, u32[]{:S(2)}, u32[]{:S(2)}) async-start(bf16[128,4,256]{0,2,1:T(8,128)(2,1)} %bitcast.19), calls=%async_computation.4 | async-start | bytes 524288 | tf_op jit(solution)/shard_map/all_to_all | solution.py:86
  42.6 2.1 %copy.31 = bf16[1,128,2048]{1,2,0:T(8,128)(2,1)} copy(bf16[1,128,2048]{2,1,0:T(8,128)(2,1)} %param.11) | data formatting | bytes 1048576 | tf_op args[2]
  44.7 4.7 %all-to-all-done.4 = bf16[128,4,256]{0,2,1:T(8,128)(2,1)S(1)} async-done(((bf16[128,4,256]{0,2,1:T(8,128)(2,1)}), bf16[128,4,256]{0,2,1:T(8,128)(2,1)S(1)}, u32[]{:S(2)}, u32[]{:S(2)}) %all-to-all-start.4) | async-done | bytes 262176 | tf_op jit(solution)/shard_map/all_to_all | solution.py:86
  49.4 3.5 %all-to-all-start.3 = ((bf16[128,4,512]{0,2,1:T(8,128)(2,1)}), bf16[128,4,512]{0,2,1:T(8,128)(2,1)S(1)}, u32[]{:S(2)}, u32[]{:S(2)}) async-start(bf16[128,4,512]{0,2,1:T(8,128)(2,1)} %bitcast.15), calls=%async_computation.3 | async-start | bytes 1048576 | tf_op jit(solution)/shard_map/all_to_all | solution.py:90
  52.9 10.2 %all-to-all-done.3 = bf16[128,4,512]{0,2,1:T(8,128)(2,1)S(1)} async-done(((bf16[128,4,512]{0,2,1:T(8,128)(2,1)}), bf16[128,4,512]{0,2,1:T(8,128)(2,1)S(1)}, u32[]{:S(2)}, u32[]{:S(2)}) %all-to-all-start.3) | async-done | bytes 524320 | tf_op jit(solution)/shard_map/all_to_all | solution.py:90
  63.1 32.2 %while.17 = (s32[]{:T(128)}, f32[256,512]{1,0:T(8,128)S(1)}, f32[256]{0:T(256)S(1)}, f32[]{:T(128)}, bf16[4,128,512]{1,2,0:T(8,128)(2,1)}, /*index=5*/f32[4,128]...) while((s32[]{:T(128)}, f32[256,512]{1,0:T(8,128)S(1)}, ...), condition=%wide.region_5.6_spmd.clone, body=%wide.region_0.5_spmd.clone.sunk | while | flops 555633152 | bytes 3825425 | solution.py:63
  63.4 0.6 slice.7
  64.0 0.8 subtract_reduce_fusion.2
  64.7 1.3 %fusion.87 = (f32[]{:T(128)}, f32[128]{0:T(128)S(1)}) fusion(f32[128]{0:T(128)S(1)} %get-tuple-element.231, f32[]{:T(128)} %bitcast.142, f32[4,128]{1,0:T(4,128)S(1)} %get-tuple-element.274, s32[]{:T(128)} %get-tuple-element.255), kind=kLoop, calls=%fused_computation.63.clone.1 | loop fusion | flops 383 | bytes 1548 | tf_op jit(solution)/shard_map/while/body/eval_jaxpr/reduce_max | solution.py:43
  67.9 0.7 subtract_exponential_fusion.2
  69.3 0.4 fusion.93
  69.8 0.7 constant_dynamic-update-slice_fusion.2
  70.5 0.6 convolution_add_fusion.2
  71.4 0.6 slice.7
  72.0 0.8 subtract_reduce_fusion.2
  72.8 1.3 %fusion.87 = (f32[]{:T(128)}, f32[128]{0:T(128)S(1)}) fusion(f32[128]{0:T(128)S(1)} %get-tuple-element.231, f32[]{:T(128)} %bitcast.142, f32[4,128]{1,0:T(4,128)S(1)} %get-tuple-element.274, s32[]{:T(128)} %get-tuple-element.255), kind=kLoop, calls=%fused_computation.63.clone.1 | loop fusion | flops 383 | bytes 1548 | tf_op jit(solution)/shard_map/while/body/eval_jaxpr/reduce_max | solution.py:43
  76.0 0.7 subtract_exponential_fusion.2
  77.4 0.4 fusion.93
  77.9 0.7 constant_dynamic-update-slice_fusion.2
  78.5 0.6 convolution_add_fusion.2
  79.5 0.6 slice.7
  80.0 0.8 subtract_reduce_fusion.2
  80.8 1.3 %fusion.87 = (f32[]{:T(128)}, f32[128]{0:T(128)S(1)}) fusion(f32[128]{0:T(128)S(1)} %get-tuple-element.231, f32[]{:T(128)} %bitcast.142, f32[4,128]{1,0:T(4,128)S(1)} %get-tuple-element.274, s32[]{:T(128)} %get-tuple-element.255), kind=kLoop, calls=%fused_computation.63.clone.1 | loop fusion | flops 383 | bytes 1548 | tf_op jit(solution)/shard_map/while/body/eval_jaxpr/reduce_max | solution.py:43
  84.0 0.7 subtract_exponential_fusion.2
  85.4 0.4 fusion.93
  85.9 0.7 constant_dynamic-update-slice_fusion.2
  86.6 0.6 convolution_add_fusion.2
  87.5 0.6 slice.7
  88.1 0.8 subtract_reduce_fusion.2
  88.9 1.3 %fusion.87 = (f32[]{:T(128)}, f32[128]{0:T(128)S(1)}) fusion(f32[128]{0:T(128)S(1)} %get-tuple-element.231, f32[]{:T(128)} %bitcast.142, f32[4,128]{1,0:T(4,128)S(1)} %get-tuple-element.274, s32[]{:T(128)} %get-tuple-element.255), kind=kLoop, calls=%fused_computation.63.clone.1 | loop fusion | flops 383 | bytes 1548 | tf_op jit(solution)/shard_map/while/body/eval_jaxpr/reduce_max | solution.py:43
  92.0 0.7 subtract_exponential_fusion.2
  93.4 0.4 fusion.93
  94.0 0.7 constant_dynamic-update-slice_fusion.2
  94.6 0.6 convolution_add_fusion.2
  95.2 3.5 %all-to-all-start.5 = ((bf16[4,128,512]{1,2,0:T(8,128)(2,1)}), bf16[4,128,512]{1,2,0:T(8,128)(2,1)S(1)}, u32[]{:S(2)}, u32[]{:S(2)}) async-start(bf16[4,128,512]{1,2,0:T(8,128)(2,1)} %get-tuple-element.62), calls=%async_computation.5 | async-start | bytes 1048576 | tf_op jit(solution)/shard_map/all_to_all | solution.py:108
  99.0 10.0 %all-to-all-done.5 = bf16[4,128,512]{1,2,0:T(8,128)(2,1)S(1)} async-done(((bf16[4,128,512]{1,2,0:T(8,128)(2,1)}), bf16[4,128,512]{1,2,0:T(8,128)(2,1)S(1)}, u32[]{:S(2)}, u32[]{:S(2)}) %all-to-all-start.5) | async-done | bytes 524320 | tf_op jit(solution)/shard_map/all_to_all | solution.py:108
  109.3 5.5 %fusion.49 = bf16[1,128,2048]{2,1,0:T(8,128)(2,1)} fusion(bf16[128,2048]{0,1:T(8,128)(2,1)S(1)} %fusion.50, bf16[2048,2048]{1,0:T(8,128)(2,1)} %all-gather.2.cloned.1.call-done), kind=kOutput, calls=%fused_computation.65 | convolution fusion | flops 1074003968 | bytes 9437184 | tf_op jit(solution)/shard_map/dot_general | solution.py:112
  (60 shorter events, 6.7 us)
Async XLA Ops:
  6.5 102.8 %all-gather.2.cloned.1.call-start = ((), (), s32[]{:S(2)}) async-start(), calls=%async_computation.6 | async-start | bytes 9437184 | tf_op jit(solution)/shard_map/all_gather | solution.py:114
  8.5 11.8 %all-to-all-start = ((bf16[128,4,1]{0,2,1:T(2,128)(2,1)}), bf16[128,4,1]{0,2,1:T(2,128)(2,1)S(1)}, u32[]{:S(2)}, u32[]{:S(2)}) async-start(bf16[128,4,1]{0,2,1:T(2,128)(2,1)} %copy.28), calls=%async_computation | async-start | bytes 4096 | tf_op jit(solution)/shard_map/all_to_all | solution.py:98
  20.4 8.6 %all-to-all-start.1 = ((bf16[128,4,1]{0,2,1:T(2,128)(2,1)}), bf16[128,4,1]{0,2,1:T(2,128)(2,1)S(1)}, u32[]{:S(2)}, u32[]{:S(2)}) async-start(bf16[128,4,1]{0,2,1:T(2,128)(2,1)} %copy.29), calls=%async_computation.1 | async-start | bytes 4096 | tf_op jit(solution)/shard_map/all_to_all | solution.py:97
  29.0 10.2 %all-to-all-start.2 = ((bf16[128,4,256]{0,2,1:T(8,128)(2,1)}), bf16[128,4,256]{0,2,1:T(8,128)(2,1)S(1)}, u32[]{:S(2)}, u32[]{:S(2)}) async-start(bf16[128,4,256]{0,2,1:T(8,128)(2,1)} %bitcast.11), calls=%async_computation.2 | async-start | bytes 524288 | tf_op jit(solution)/shard_map/all_to_all | solution.py:87
  39.1 10.2 %all-to-all-start.4 = ((bf16[128,4,256]{0,2,1:T(8,128)(2,1)}), bf16[128,4,256]{0,2,1:T(8,128)(2,1)S(1)}, u32[]{:S(2)}, u32[]{:S(2)}) async-start(bf16[128,4,256]{0,2,1:T(8,128)(2,1)} %bitcast.19), calls=%async_computation.4 | async-start | bytes 524288 | tf_op jit(solution)/shard_map/all_to_all | solution.py:86
  49.4 13.7 %all-to-all-start.3 = ((bf16[128,4,512]{0,2,1:T(8,128)(2,1)}), bf16[128,4,512]{0,2,1:T(8,128)(2,1)S(1)}, u32[]{:S(2)}, u32[]{:S(2)}) async-start(bf16[128,4,512]{0,2,1:T(8,128)(2,1)} %bitcast.15), calls=%async_computation.3 | async-start | bytes 1048576 | tf_op jit(solution)/shard_map/all_to_all | solution.py:90
  63.1 35.7 %copy-start = (bf16[1,128,2048]{2,1,0:T(8,128)(2,1)S(1)}, bf16[1,128,2048]{2,1,0:T(8,128)(2,1)}, u32[]{:S(2)}) copy-start(bf16[1,128,2048]{2,1,0:T(8,128)(2,1)} %param.12) | copy-start | bytes 1572868
  95.2 13.7 %all-to-all-start.5 = ((bf16[4,128,512]{1,2,0:T(8,128)(2,1)}), bf16[4,128,512]{1,2,0:T(8,128)(2,1)S(1)}, u32[]{:S(2)}, u32[]{:S(2)}) async-start(bf16[4,128,512]{1,2,0:T(8,128)(2,1)} %get-tuple-element.62), calls=%async_computation.5 | async-start | bytes 1048576 | tf_op jit(solution)/shard_map/all_to_all | solution.py:108
Sparse Core Ops, SparseCore 0:
  9.2 58.5 all-gather.1
where the time goes:
time: 122 us
  waiting for transfers between devices  38.3 us (31%)
  starting transfers between devices  23.4 us (19%)
  local copies, waits for them, and re-layouts  15 us (12%)
  between operations  13.5 us (11%)
  matrix products  12.9 us (11%)
  other arithmetic  12.7 us (10%)
  loops' own time  5.83 us (5%)
    all_to_all x1, waiting for transfers between devices, body(): lax.all_to_all(values[0].reshape(token_count, group_count, slice_width),...  10.2 us
    all_to_all x1, waiting for transfers between devices, body(): lax.all_to_all(hidden, 'sp', split_axis=0, concat_axis=1, tiled=True)  9.97 us
    all_to_all x1, starting transfers between devices, body(): lax.all_to_all(spread_gate(forget_gate), 'sp', split_axis=1, concat_axis=...  6.35 us
    unnamed x6, local copies, waits for them, and re-layouts  6 us
    another operation x1, loops' own time, memory_cell(): _, outputs = lax.scan(block_step, start_state, blocks)  5.83 us
    dot_general x1, matrix products, body(): jnp.dot(gated_rows, lax.all_gather(out_weight, 'dp', axis=1, tiled=True),...  5.46 us
    reduce_max x4, other arithmetic, block_step(): new_top = jnp.maximum(block_end + stabil, jnp.max(weight_log))  5.38 us
    all_to_all x1, waiting for transfers between devices, body(): lax.all_to_all(spread(key_rows), 'sp', split_axis=1, concat_axis=0, tiled...  4.92 us
  transfers between devices with their start and end apart: 7, of which 6 were waited for; matrix products, arithmetic and copies ran while one was open for 29% of the time, Pallas kernels for 0%

commit v1 on v0

--- a/solution.py
+++ b/solution.py
@@ -1,9 +1,48 @@
+import functools
 import jax
 import jax.numpy as jnp
 from jax import lax
 from jax.sharding import PartitionSpec as P
 
 BLOCK = 128
+
+
+def form_field(z, axis_no, state):
+    k_now = z.shape
+    current_value = z.reshape(
+        *k_now[:axis_no], state, k_now[axis_no] // state, *k_now[axis_no + 1 :]
+    )
+    return jnp.moveaxis(current_value, axis_no, 0)
+
+
+def refer_slots(patch, which_dim):
+    patch = jnp.moveaxis(patch, 0, which_dim)
+    spare = patch.shape
+    return patch.reshape(
+        *spare[:which_dim], spare[which_dim] * spare[which_dim + 1], *spare[which_dim + 2 :]
+    )
+
+
+def see_sample(target, which_axis, inp, original):
+    found_now = lax.axis_size(which_axis)
+    arr_next = lax.axis_index(which_axis)
+    d_next, lower = (found_now, arr_next)
+    b_now = form_field(target, inp, d_next)
+    nodes = [b_now[lower]]
+    k0 = 1
+    while k0 < d_next:
+        v_now = b_now[(lower + k0) % d_next]
+        out_arr = lax.ppermute(
+            v_now, axis_name=which_axis, perm=[(m, (m + k0) % d_next) for m in range(d_next)]
+        )
+        nodes.append(out_arr)
+        k0 = k0 + 1
+    even = jnp.stack(nodes)
+    b_now = even[(lower - jnp.arange(d_next)) % d_next]
+    return refer_slots(b_now, original)
+
+
+_measure_shelves = functools.partial(see_sample, which_axis="sp", inp=1, original=0)
 
 
 def memory_cell(query_rows, key_in, value_rows, input_log, forget_log):
@@ -95,7 +134,7 @@
             tiled=True,
         ),
         lax.all_to_all(spread_gate(input_gate), "sp", split_axis=1, concat_axis=0, tiled=True),
-        lax.all_to_all(spread_gate(forget_gate), "sp", split_axis=1, concat_axis=0, tiled=True),
+        _measure_shelves(spread_gate(forget_gate)),
     )
     output = memory_cell(
         query_all[:, 0],

time: 122 us -> 115 us (0.943)
  waiting for transfers between devices: 38.3 us -> 29.4 us
  starting transfers between devices: 23.4 us -> 25 us
    all_to_all x1, waiting for transfers between devices: 10.2 us -> 0.01 us  [body(): lax.all_to_all(values[0].reshape(token_count, group_count, slice_width),...]
    all_to_all x1 -> x0, starting transfers between devices: 6.35 us -> none  [body(): lax.all_to_all(spread_gate(forget_gate), 'sp', split_axis=1, concat_axis=...]
    ppermute x0 -> x3, waiting for transfers between devices: none -> 5.05 us  [see_sample(): lax.ppermute(v_now, axis_name=which_axis, perm=[(m, (m + k0) % d_next) fo...]
    ppermute x0 -> x3, starting transfers between devices: none -> 4.86 us  [see_sample(): lax.ppermute(v_now, axis_name=which_axis, perm=[(m, (m + k0) % d_next) fo...]
    all_to_all x1 -> x0, waiting for transfers between devices: 4.22 us -> none  [body(): lax.all_to_all(spread_gate(forget_gate), 'sp', split_axis=1, concat_axis=...]
    all_to_all x1, starting transfers between devices: 3.23 us -> 6.35 us  [body(): lax.all_to_all(spread_gate(input_gate), 'sp', split_axis=1, concat_axis=0...]
    all_to_all x1 -> x0, local copies, waits for them, and re-layouts: 1.26 us -> none  [body(): lax.all_to_all(spread_gate(forget_gate), 'sp', split_axis=1, concat_axis=...]
  transfers between devices with their start and end apart: 7 -> 9, of which waited for: 6 -> 7; matrix products, arithmetic and copies ran while one was open for 29% -> 30% of each run, Pallas kernels for 0% -> 0%
where the time goes in v1:
time: 115 us; the launch traced here: 114 us
  waiting for transfers between devices  29.4 us (26%)
  starting transfers between devices  25 us (22%)
  local copies, waits for them, and re-layouts  14.9 us (13%)
  between operations  13.6 us (12%)
  matrix products  12.9 us (11%)
  other arithmetic  12.3 us (11%)
  loops' own time  5.87 us (5%)
    all_to_all x1, waiting for transfers between devices, body(): lax.all_to_all(hidden, 'sp', split_axis=0, concat_axis=1, tiled=True)  9.97 us
    all_to_all x1, starting transfers between devices, body(): lax.all_to_all(spread_gate(input_gate), 'sp', split_axis=1, concat_axis=0...  6.35 us
    unnamed x6, local copies, waits for them, and re-layouts  5.96 us
    another operation x1, loops' own time, memory_cell(): _, outputs = lax.scan(block_step, start_state, blocks)  5.87 us
    dot_general x1, matrix products, body(): jnp.dot(gated_rows, lax.all_gather(out_weight, 'dp', axis=1, tiled=True),...  5.46 us
    reduce_max x4, other arithmetic, block_step(): new_top = jnp.maximum(block_end + stabil, jnp.max(weight_log))  5.23 us
    all_to_all x1, waiting for transfers between devices, body(): lax.all_to_all(spread(key_rows), 'sp', split_axis=1, concat_axis=0, tiled...  5.22 us
    ppermute x3, waiting for transfers between devices, see_sample(): lax.ppermute(v_now, axis_name=which_axis, perm=[(m, (m + k0) % d_next) fo...  5.05 us
  transfers between devices with their start and end apart: 9, of which 7 were waited for; matrix products, arithmetic and copies ran while one was open for 30% of the time, Pallas kernels for 0%

profile of v1, /device:TPU:0, one launch (start us, length us, event | category | flops | bytes accessed | tf_op | source)
XLA Modules:
  0.0 113.9 jit_solution(518766541164611768)
XLA Ops:
  6.5 0.7 all-gather.2.cloned.1.call-update
  7.3 1.3 %copy.44 = bf16[128,4,1]{0,2,1:T(2,128)(2,1)} copy(bf16[128,4,1]{0,1,2:T(4,128)(2,1)} %bitcast.166) | data formatting | bytes 2048 | tf_op jit(solution)/shard_map/all_to_all | solution.py:136
  8.5 6.3 %all-to-all-start = ((bf16[128,4,1]{0,2,1:T(2,128)(2,1)}), bf16[128,4,1]{0,2,1:T(2,128)(2,1)S(1)}, u32[]{:S(2)}, u32[]{:S(2)}) async-start(bf16[128,4,1]{0,2,1:T(2,128)(2,1)} %copy.44), calls=%async_computation | async-start | bytes 4096 | tf_op jit(solution)/shard_map/all_to_all | solution.py:136
  14.9 1.8 %copy.45 = bf16[1,128,1024]{1,2,0:T(8,128)(2,1)} copy(bf16[1,128,1024]{2,1,0:T(8,128)(2,1)} %param.10) | data formatting | bytes 524288 | tf_op args[1]
  16.7 3.8 %all-to-all-done = bf16[128,4,1]{0,2,1:T(2,128)(2,1)S(1)} async-done(((bf16[128,4,1]{0,2,1:T(2,128)(2,1)}), bf16[128,4,1]{0,2,1:T(2,128)(2,1)S(1)}, u32[]{:S(2)}, u32[]{:S(2)}) %all-to-all-start) | async-done | bytes 1056 | tf_op jit(solution)/shard_map/all_to_all | solution.py:136
  20.4 3.4 %all-to-all-start.1 = ((bf16[128,4,256]{0,2,1:T(8,128)(2,1)}), bf16[128,4,256]{0,2,1:T(8,128)(2,1)S(1)}, u32[]{:S(2)}, u32[]{:S(2)}) async-start(bf16[128,4,256]{0,2,1:T(8,128)(2,1)} %bitcast.18), calls=%async_computation.1 | async-start | bytes 524288 | tf_op jit(solution)/shard_map/all_to_all | solution.py:126
  23.9 1.8 %copy.47 = bf16[1,128,1024]{1,2,0:T(8,128)(2,1)} copy(bf16[1,128,1024]{2,1,0:T(8,128)(2,1)} %param.9) | data formatting | bytes 524288 | tf_op args[0]
  25.7 5.2 %all-to-all-done.1 = bf16[128,4,256]{0,2,1:T(8,128)(2,1)S(1)} async-done(((bf16[128,4,256]{0,2,1:T(8,128)(2,1)}), bf16[128,4,256]{0,2,1:T(8,128)(2,1)S(1)}, u32[]{:S(2)}, u32[]{:S(2)}) %all-to-all-start.1) | async-done | bytes 262176 | tf_op jit(solution)/shard_map/all_to_all | solution.py:126
  30.9 3.4 %all-to-all-start.3 = ((bf16[128,4,256]{0,2,1:T(8,128)(2,1)}), bf16[128,4,256]{0,2,1:T(8,128)(2,1)S(1)}, u32[]{:S(2)}, u32[]{:S(2)}) async-start(bf16[128,4,256]{0,2,1:T(8,128)(2,1)} %bitcast.26), calls=%async_computation.3 | async-start | bytes 524288 | tf_op jit(solution)/shard_map/all_to_all | solution.py:125
  34.3 2.1 %copy.46 = bf16[1,128,2048]{1,2,0:T(8,128)(2,1)} copy(bf16[1,128,2048]{2,1,0:T(8,128)(2,1)} %param.11) | data formatting | bytes 1048576 | tf_op args[2]
  36.4 4.7 %all-to-all-done.3 = bf16[128,4,256]{0,2,1:T(8,128)(2,1)S(1)} async-done(((bf16[128,4,256]{0,2,1:T(8,128)(2,1)}), bf16[128,4,256]{0,2,1:T(8,128)(2,1)S(1)}, u32[]{:S(2)}, u32[]{:S(2)}) %all-to-all-start.3) | async-done | bytes 262176 | tf_op jit(solution)/shard_map/all_to_all | solution.py:125
  41.1 3.5 %all-to-all-start.2 = ((bf16[128,4,512]{0,2,1:T(8,128)(2,1)}), bf16[128,4,512]{0,2,1:T(8,128)(2,1)S(1)}, u32[]{:S(2)}, u32[]{:S(2)}) async-start(bf16[128,4,512]{0,2,1:T(8,128)(2,1)} %bitcast.22), calls=%async_computation.2 | async-start | bytes 1048576 | tf_op jit(solution)/shard_map/all_to_all | solution.py:129
  44.6 0.8 fusion.58
  45.4 3.7 %collective-permute-start.2 = (bf16[128,1]{0,1:T(2,128)(2,1)S(1)}, bf16[128,1]{0,1:T(2,128)(2,1)S(1)}, u32[]{:S(2)}, u32[]{:S(2)}) collective-permute-start(bf16[128,1]{0,1:T(2,128)(2,1)S(1)} %get-tuple-element.161), channel_id=1, source_target_pairs={{0,24},{8,0},{16,8},{24,16},{1,25},{9,1},{17,9},{25,17},{2,26},{10... | collective-permute-start | bytes 776 | tf_op jit(solution)/shard_map/ppermute | solution.py:35
  49.2 1.1 collective-permute-start.1
  50.5 4.1 %collective-permute-done = bf16[128,1]{0,1:T(2,128)(2,1)S(1)} collective-permute-done((bf16[128,1]{0,1:T(2,128)(2,1)S(1)}, bf16[128,1]{0,1:T(2,128)(2,1)S(1)}, u32[]{:S(2)}, u32[]{:S(2)}) %collective-permute-start) | collective-permute-done | bytes 288 | tf_op jit(solution)/shard_map/ppermute | solution.py:35
  54.5 0.8 collective-permute-done.1
  55.4 0.6 gather_fusion
  56.0 31.5 %while.17 = (s32[]{:T(128)}, f32[256,512]{1,0:T(8,128)S(1)}, f32[256]{0:T(256)S(1)}, f32[]{:T(128)}, bf16[4,128,512]{1,2,0:T(8,128)(2,1)}, /*index=5*/f32[4,128]...) while((s32[]{:T(128)}, f32[256,512]{1,0:T(8,128)S(1)}, ...), condition=%wide.region_5.6_spmd.clone, body=%wide.region_0.5_spmd.clone.sunk | while | flops 555633152 | bytes 3825425 | solution.py:102
  56.3 0.5 slice.9
  56.9 0.7 subtract_reduce_fusion.2
  57.6 1.3 %fusion.99 = (f32[]{:T(128)}, f32[128]{0:T(128)S(1)}) fusion(f32[128]{0:T(128)S(1)} %get-tuple-element.235, f32[]{:T(128)} %bitcast.157, f32[4,128]{1,0:T(4,128)S(1)} %get-tuple-element.278, s32[]{:T(128)} %get-tuple-element.259), kind=kLoop, calls=%fused_computation.64.clone.1 | loop fusion | flops 383 | bytes 1548 | tf_op jit(solution)/shard_map/while/body/eval_jaxpr/reduce_max | solution.py:82
  60.7 0.6 subtract_exponential_fusion.2
  62.1 0.4 fusion.105
  62.6 0.7 constant_dynamic-update-slice_fusion.2
  63.3 0.6 convolution_add_fusion.2
  64.2 0.5 slice.9
  64.7 0.7 subtract_reduce_fusion.2
  65.5 1.3 %fusion.99 = (f32[]{:T(128)}, f32[128]{0:T(128)S(1)}) fusion(f32[128]{0:T(128)S(1)} %get-tuple-element.235, f32[]{:T(128)} %bitcast.157, f32[4,128]{1,0:T(4,128)S(1)} %get-tuple-element.278, s32[]{:T(128)} %get-tuple-element.259), kind=kLoop, calls=%fused_computation.64.clone.1 | loop fusion | flops 383 | bytes 1548 | tf_op jit(solution)/shard_map/while/body/eval_jaxpr/reduce_max | solution.py:82
  68.6 0.6 subtract_exponential_fusion.2
  70.0 0.4 fusion.105
  70.5 0.7 constant_dynamic-update-slice_fusion.2
  71.2 0.6 convolution_add_fusion.2
  72.1 0.5 slice.9
  72.6 0.7 subtract_reduce_fusion.2
  73.4 1.3 %fusion.99 = (f32[]{:T(128)}, f32[128]{0:T(128)S(1)}) fusion(f32[128]{0:T(128)S(1)} %get-tuple-element.235, f32[]{:T(128)} %bitcast.157, f32[4,128]{1,0:T(4,128)S(1)} %get-tuple-element.278, s32[]{:T(128)} %get-tuple-element.259), kind=kLoop, calls=%fused_computation.64.clone.1 | loop fusion | flops 383 | bytes 1548 | tf_op jit(solution)/shard_map/while/body/eval_jaxpr/reduce_max | solution.py:82
  76.5 0.6 subtract_exponential_fusion.2
  78.4 0.7 constant_dynamic-update-slice_fusion.2
  79.1 0.6 convolution_add_fusion.2
  80.0 0.5 slice.9
  80.5 0.7 subtract_reduce_fusion.2
  81.3 1.3 %fusion.99 = (f32[]{:T(128)}, f32[128]{0:T(128)S(1)}) fusion(f32[128]{0:T(128)S(1)} %get-tuple-element.235, f32[]{:T(128)} %bitcast.157, f32[4,128]{1,0:T(4,128)S(1)} %get-tuple-element.278, s32[]{:T(128)} %get-tuple-element.259), kind=kLoop, calls=%fused_computation.64.clone.1 | loop fusion | flops 383 | bytes 1548 | tf_op jit(solution)/shard_map/while/body/eval_jaxpr/reduce_max | solution.py:82
  84.4 0.6 subtract_exponential_fusion.2
  86.3 0.7 constant_dynamic-update-slice_fusion.2
  86.9 0.6 convolution_add_fusion.2
  87.6 3.5 %all-to-all-start.4 = ((bf16[4,128,512]{1,2,0:T(8,128)(2,1)}), bf16[4,128,512]{1,2,0:T(8,128)(2,1)S(1)}, u32[]{:S(2)}, u32[]{:S(2)}) async-start(bf16[4,128,512]{1,2,0:T(8,128)(2,1)} %get-tuple-element.62), calls=%async_computation.4 | async-start | bytes 1048576 | tf_op jit(solution)/shard_map/all_to_all | solution.py:147
  91.3 10.0 %all-to-all-done.4 = bf16[4,128,512]{1,2,0:T(8,128)(2,1)S(1)} async-done(((bf16[4,128,512]{1,2,0:T(8,128)(2,1)}), bf16[4,128,512]{1,2,0:T(8,128)(2,1)S(1)}, u32[]{:S(2)}, u32[]{:S(2)}) %all-to-all-start.4) | async-done | bytes 524320 | tf_op jit(solution)/shard_map/all_to_all | solution.py:147
  101.6 5.5 %fusion.49 = bf16[1,128,2048]{2,1,0:T(8,128)(2,1)} fusion(bf16[128,2048]{0,1:T(8,128)(2,1)S(1)} %fusion.50, bf16[2048,2048]{1,0:T(8,128)(2,1)} %all-gather.2.cloned.1.call-done), kind=kOutput, calls=%fused_computation.66 | convolution fusion | flops 1074003968 | bytes 9437184 | tf_op jit(solution)/shard_map/dot_general | solution.py:151
  (67 shorter events, 7.7 us)
Async XLA Ops:
  6.5 95.1 %all-gather.2.cloned.1.call-start = ((), (), s32[]{:S(2)}) async-start(), calls=%async_computation.5 | async-start | bytes 9437184 | tf_op jit(solution)/shard_map/all_gather | solution.py:153
  8.5 11.9 %all-to-all-start = ((bf16[128,4,1]{0,2,1:T(2,128)(2,1)}), bf16[128,4,1]{0,2,1:T(2,128)(2,1)S(1)}, u32[]{:S(2)}, u32[]{:S(2)}) async-start(bf16[128,4,1]{0,2,1:T(2,128)(2,1)} %copy.44), calls=%async_computation | async-start | bytes 4096 | tf_op jit(solution)/shard_map/all_to_all | solution.py:136
  20.4 10.5 %all-to-all-start.1 = ((bf16[128,4,256]{0,2,1:T(8,128)(2,1)}), bf16[128,4,256]{0,2,1:T(8,128)(2,1)S(1)}, u32[]{:S(2)}, u32[]{:S(2)}) async-start(bf16[128,4,256]{0,2,1:T(8,128)(2,1)} %bitcast.18), calls=%async_computation.1 | async-start | bytes 524288 | tf_op jit(solution)/shard_map/all_to_all | solution.py:126
  30.9 10.2 %all-to-all-start.3 = ((bf16[128,4,256]{0,2,1:T(8,128)(2,1)}), bf16[128,4,256]{0,2,1:T(8,128)(2,1)S(1)}, u32[]{:S(2)}, u32[]{:S(2)}) async-start(bf16[128,4,256]{0,2,1:T(8,128)(2,1)} %bitcast.26), calls=%async_computation.3 | async-start | bytes 524288 | tf_op jit(solution)/shard_map/all_to_all | solution.py:125
  41.1 14.9 %all-to-all-start.2 = ((bf16[128,4,512]{0,2,1:T(8,128)(2,1)}), bf16[128,4,512]{0,2,1:T(8,128)(2,1)S(1)}, u32[]{:S(2)}, u32[]{:S(2)}) async-start(bf16[128,4,512]{0,2,1:T(8,128)(2,1)} %bitcast.22), calls=%async_computation.2 | async-start | bytes 1048576 | tf_op jit(solution)/shard_map/all_to_all | solution.py:129
  45.4 5.0 %collective-permute-start.2 = (bf16[128,1]{0,1:T(2,128)(2,1)S(1)}, bf16[128,1]{0,1:T(2,128)(2,1)S(1)}, u32[]{:S(2)}, u32[]{:S(2)}) collective-permute-start(bf16[128,1]{0,1:T(2,128)(2,1)S(1)} %get-tuple-element.161), channel_id=1, source_target_pairs={{0,24},{8,0},{16,8},{24,16},{1,25},{9,1},{17,9},{25,17},{2,26},{10... | collective-permute-start | bytes 776 | tf_op jit(solution)/shard_map/ppermute | solution.py:35
  49.2 5.4 %collective-permute-start = (bf16[128,1]{0,1:T(2,128)(2,1)S(1)}, bf16[128,1]{0,1:T(2,128)(2,1)S(1)}, u32[]{:S(2)}, u32[]{:S(2)}) collective-permute-start(bf16[128,1]{0,1:T(2,128)(2,1)S(1)} %get-tuple-element.160), channel_id=1, source_target_pairs={{0,8},{8,16},{16,24},{24,0},{1,9},{9,17},{17,25},{25,1},{2,10},{10... | collective-permute-start | bytes 776 | tf_op jit(solution)/shard_map/ppermute | solution.py:35
  49.2 6.2 %collective-permute-start.1 = (bf16[128,1]{0,1:T(2,128)(2,1)S(1)}, bf16[128,1]{0,1:T(2,128)(2,1)S(1)}, u32[]{:S(2)}, u32[]{:S(2)}) collective-permute-start(bf16[128,1]{0,1:T(2,128)(2,1)S(1)} %get-tuple-element.162), channel_id=1, source_target_pairs={{0,16},{8,24},{16,0},{24,8},{1,17},{9,25},{17,1},{25,9},{2,18},{10... | collective-permute-start | bytes 776 | tf_op jit(solution)/shard_map/ppermute | solution.py:35
  56.0 35.0 %copy-start = (bf16[1,128,2048]{2,1,0:T(8,128)(2,1)S(1)}, bf16[1,128,2048]{2,1,0:T(8,128)(2,1)}, u32[]{:S(2)}) copy-start(bf16[1,128,2048]{2,1,0:T(8,128)(2,1)} %param.12) | copy-start | bytes 1572868
  87.6 13.7 %all-to-all-start.4 = ((bf16[4,128,512]{1,2,0:T(8,128)(2,1)}), bf16[4,128,512]{1,2,0:T(8,128)(2,1)S(1)}, u32[]{:S(2)}, u32[]{:S(2)}) async-start(bf16[4,128,512]{1,2,0:T(8,128)(2,1)} %get-tuple-element.62), calls=%async_computation.4 | async-start | bytes 1048576 | tf_op jit(solution)/shard_map/all_to_all | solution.py:147
Sparse Core Ops, SparseCore 0:
  9.2 58.5 all-gather.1
